TPU v7x, 32 devices: a whole 2x2x4 slice. The times are simulated.
32 devices in a mesh: ep: 4 (over y, x), tp: 8 (over z, core).
Axes of the slice: x: 2, y: 2, z: 4, core: 2. Of those that a mesh axis runs over, the one named last changes fastest.
Arguments:
- q_latent: bfloat16 [4096, 512], P('ep'), may hold values from -6 to 6
- kv_latent: bfloat16 [4096, 256], P('ep'), may hold values from -6 to 6
- rope_key: bfloat16 [4096, 32], P('ep'), may hold values from -1200 to 1200
- q_gain: float32 [512], replicated, may hold values from 0.1 to 1.9
- kv_gain: float32 [256], replicated, may hold values from 0.1 to 1.9
- w_query: bfloat16 [512, 1536], P(None, 'tp'), may hold values from -0.25 to 0.25
- w_keyval: bfloat16 [256, 2048], P(None, 'tp'), may hold values from -0.375 to 0.375
- w_output: bfloat16 [1024, 2048], P(None, 'tp'), may hold values from -0.1875 to 0.1875
- moe_input: bfloat16 [1024, 2048], P('ep'), may hold values from -6 to 6
- moe_gain: float32 [2048], replicated, may hold values from 0.1 to 1.9
- routes: int32 [1024, 2], P('ep'), may hold values from 0 to 3, all different within a row; in each aligned block of 32 rows (0 to 31, 32 to 63, ...) at most 24 rows name the same one
- route_weight: float32 [1024, 2], P('ep'), may hold values from 0.25 to 2
- expert_gate: bfloat16 [4, 2048, 4096], P('ep', None, 'tp'), may hold values from -0.125 to 0.125
- expert_up: bfloat16 [4, 2048, 4096], P('ep', None, 'tp'), may hold values from -0.125 to 0.125
- expert_down: bfloat16 [4, 4096, 2048], P('ep', 'tp'), may hold values from -0.09375 to 0.09375
- shared_gate: bfloat16 [2048, 2048], P(None, 'tp'), may hold values from -0.125 to 0.125
- shared_up: bfloat16 [2048, 2048], P(None, 'tp'), may hold values from -0.125 to 0.125
- shared_down: bfloat16 [2048, 2048], P('tp'), may hold values from -0.125 to 0.125
Outputs:
- mixed: bfloat16 [4096, 2048], P('ep', 'tp')
- moe_out: bfloat16 [1024, 2048], P(('ep', 'tp'))
Inputs may be any that keep to these rules, and one draw needn't show every extreme that they name: `routes`: in each aligned block of 32 rows (the rows of one device's output) no expert is named by more than 24 rows, a bound that some block reaches. Each row names 2 different experts.
All inputs are finite; a program needn't handle non-finite values.
Results may differ from a plain program's by a relative error of at most 0.023.
Values may be sent and summed in bfloat16 or wider, within the bound.
A program may use at most 128 MiB of HBM per device.

v0:
```python
import jax
import jax.numpy as jnp
from jax import lax
from jax.sharding import PartitionSpec as P

NOPE = 64
ROPE_DIM = 32
VDIM = 64
MOE_DEV = 32
norm_eps = 1e-06
layer_eps = 1e-05
rotary_base = 10000.0
floor_value = -1e30


def rms_scale(values, gain):
    widened = values.astype(jnp.float32)
    return (
        widened * lax.rsqrt(jnp.mean(widened * widened, -1, keepdims=True) + norm_eps) * gain
    ).astype(jnp.bfloat16)


def layer_scale(values, gain):
    widened = values.astype(jnp.float32)
    centred = widened - jnp.mean(widened, -1, keepdims=True)
    return (
        centred * lax.rsqrt(jnp.mean(centred * centred, -1, keepdims=True) + layer_eps) * gain
    ).astype(jnp.bfloat16)


def rotary_tables(positions):
    halfway = ROPE_DIM // 2
    inverse = rotary_base ** (-(jnp.arange(halfway, dtype=jnp.float32) * 2.0 / ROPE_DIM))
    angles = positions.astype(jnp.float32)[:, None] * inverse[None, :]
    return (jnp.cos(angles), jnp.sin(angles))


def rotate(values, cosine_table, sine_table):
    halfway = values.shape[-1] // 2
    first_half = values[..., :halfway]
    second_half = values[..., halfway:]
    return jnp.concatenate(
        [
            first_half * cosine_table - second_half * sine_table,
            second_half * cosine_table + first_half * sine_table,
        ],
        -1,
    )


def block_stats(query_block, query_pos, keyvals, rotated_keys, key_pos):
    scale = float(NOPE + ROPE_DIM) ** (-0.5)
    scores = jnp.einsum(
        "qhd,khd->hqk",
        query_block[..., :NOPE],
        keyvals[..., :NOPE],
        preferred_element_type=jnp.float32,
    )
    scores = (
        scores
        + jnp.einsum(
            "qhd,kd->hqk", query_block[..., NOPE:], rotated_keys, preferred_element_type=jnp.float32
        )
    ) * scale
    allowed = key_pos[None, :] <= query_pos[:, None]
    scores = jnp.where(allowed[None], scores, -jnp.inf)
    block_max = jnp.max(scores, -1)
    weights = jnp.exp(scores - block_max[..., None])
    block_sum = jnp.sum(weights, -1)
    attended = jnp.einsum(
        "hqk,khd->qhd",
        weights.astype(jnp.bfloat16),
        keyvals[..., NOPE:],
        preferred_element_type=jnp.float32,
    ).astype(jnp.bfloat16)
    return (block_max.T, block_sum.T, attended)


def merge_block(carried, stats):
    running_max, running_sum, running_acc = carried
    block_max, block_sum, attended = stats
    new_max = jnp.maximum(running_max, block_max)
    old_weight = jnp.exp(running_max - new_max)
    new_weight = jnp.exp(block_max - new_max)
    return (
        new_max,
        running_sum * old_weight + block_sum * new_weight,
        running_acc * old_weight[..., None] + attended.astype(jnp.float32) * new_weight[..., None],
    )


def body(
    q_latent,
    kv_latent,
    rope_key,
    q_gain,
    kv_gain,
    w_query,
    w_keyval,
    w_output,
    moe_input,
    moe_gain,
    routes,
    route_weight,
    expert_gate,
    expert_up,
    expert_down,
    shared_gate,
    shared_up,
    shared_down,
):
    row_count = q_latent.shape[0]
    own_index = lax.axis_index("ep")
    ep_count = lax.axis_size("ep")
    tp_count = lax.axis_size("tp")
    positions = own_index * row_count + jnp.arange(row_count, dtype=jnp.int32)
    cosine_table, sine_table = rotary_tables(positions)
    q_normed = rms_scale(q_latent, q_gain)
    kv_normed = rms_scale(kv_latent, kv_gain)
    key_rotated = rotate(rope_key.astype(jnp.float32), cosine_table, sine_table).astype(
        jnp.bfloat16
    )
    heads_local = w_query.shape[1] // (NOPE + ROPE_DIM)
    projected = jnp.dot(q_normed, w_query, preferred_element_type=jnp.float32)
    projected = projected.reshape(row_count, heads_local, NOPE + ROPE_DIM)
    queries = jnp.concatenate(
        [
            projected[..., :NOPE],
            rotate(projected[..., NOPE:], cosine_table[:, None, :], sine_table[:, None, :]),
        ],
        -1,
    ).astype(jnp.bfloat16)

    def expand_keys(latent_rows):
        expanded = jnp.dot(latent_rows, w_keyval, preferred_element_type=jnp.float32).astype(
            jnp.bfloat16
        )
        return expanded.reshape(latent_rows.shape[0], heads_local, NOPE + VDIM)

    initial = (
        jnp.full((row_count, heads_local), floor_value, jnp.float32),
        jnp.zeros((row_count, heads_local), jnp.float32),
        jnp.zeros((row_count, heads_local, VDIM), jnp.float32),
    )
    carried = initial
    latent_piece = lax.all_gather(kv_normed, "ep", axis=0, tiled=True)
    rotated_piece = lax.all_gather(key_rotated, "ep", axis=0, tiled=True)
    block_count = latent_piece.shape[0] // row_count

    def visit_block(inner, offset):

        def live(current):
            latent_rows = lax.dynamic_slice_in_dim(latent_piece, offset * row_count, row_count, 0)
            rotated_rows = lax.dynamic_slice_in_dim(rotated_piece, offset * row_count, row_count, 0)
            key_pos = offset * row_count + jnp.arange(row_count, dtype=jnp.int32)
            stats = block_stats(queries, positions, expand_keys(latent_rows), rotated_rows, key_pos)
            return merge_block(current, stats)

        def skipped(current):
            return current

        return (lax.cond(offset <= own_index, live, skipped, inner), None)

    carried, unused = lax.scan(visit_block, carried, jnp.arange(block_count, dtype=jnp.int32))
    running_max, running_sum, running_acc = carried
    heads_out = (
        (running_acc / running_sum[..., None])
        .astype(jnp.bfloat16)
        .reshape(row_count, heads_local * VDIM)
    )
    mixed = jnp.dot(
        lax.all_gather(heads_out, "tp", axis=1, tiled=True),
        w_output,
        preferred_element_type=jnp.float32,
    )
    mixed = mixed.astype(jnp.bfloat16)
    width = moe_input.shape[1]
    top_count = routes.shape[1]
    local_experts = expert_gate.shape[0]
    expert_count = local_experts * ep_count
    capacity = max(2, 3 * MOE_DEV * top_count // (2 * expert_count))
    normed = layer_scale(moe_input, moe_gain)
    entries = routes.reshape(tp_count, MOE_DEV * top_count)
    onehot = (entries[..., None] == jnp.arange(expert_count, dtype=jnp.int32)).astype(jnp.int32)
    earlier = jnp.cumsum(onehot, 1) - onehot
    rank_in = jnp.sum(earlier * onehot, -1)
    block_ids = jnp.arange(tp_count, dtype=jnp.int32)[:, None]
    slot_of = ((entries * tp_count + block_ids) * capacity + rank_in).reshape(-1, top_count)
    token_ids = jnp.arange(tp_count * MOE_DEV * top_count, dtype=jnp.int32) // top_count
    slot_token = (
        jnp.full((expert_count * tp_count * capacity,), -1, jnp.int32)
        .at[slot_of.reshape(-1)]
        .set(token_ids)
    )
    outgoing = jnp.where(
        (slot_token >= 0)[:, None], normed[jnp.maximum(slot_token, 0)], jnp.zeros((), jnp.bfloat16)
    )
    outgoing = outgoing.reshape(ep_count, local_experts, tp_count, capacity, width)
    arrived = lax.all_to_all(outgoing, "ep", split_axis=0, concat_axis=0, tiled=True)
    slot_rows = arrived.shape[3]
    inputs = arrived[:, 0].reshape(-1, width)
    hidden = jax.nn.silu(jnp.dot(inputs, expert_gate[0], preferred_element_type=jnp.float32))
    hidden = (hidden * jnp.dot(inputs, expert_up[0], preferred_element_type=jnp.float32)).astype(
        jnp.bfloat16
    )
    output = jnp.dot(hidden, expert_down[0], preferred_element_type=jnp.float32)
    results = [output.astype(jnp.bfloat16).reshape(ep_count, tp_count, slot_rows, width)]
    partial_value = jnp.stack(results, 1)
    shared_hidden = jax.nn.silu(jnp.dot(normed, shared_gate, preferred_element_type=jnp.float32))
    shared_hidden = (
        shared_hidden * jnp.dot(normed, shared_up, preferred_element_type=jnp.float32)
    ).astype(jnp.bfloat16)
    shared_part = jnp.dot(shared_hidden, shared_down, preferred_element_type=jnp.float32).astype(
        jnp.bfloat16
    )
    slot_total, shared_total = (
        lax.psum_scatter(
            partial_value.astype(jnp.float32).astype(jnp.bfloat16),
            "tp",
            scatter_dimension=2,
            tiled=True,
        ).astype(jnp.float32),
        lax.psum_scatter(
            shared_part.astype(jnp.float32)
            .reshape(1, 1, tp_count, MOE_DEV, width)
            .astype(jnp.bfloat16),
            "tp",
            scatter_dimension=2,
            tiled=True,
        ).astype(jnp.float32),
    )
    arrived_sums = lax.all_to_all(
        slot_total.astype(jnp.bfloat16), "ep", split_axis=0, concat_axis=0, tiled=True
    ).astype(slot_total.dtype)
    own_block = lax.axis_index("tp")
    own_entries = lax.dynamic_slice_in_dim(routes, own_block * MOE_DEV, MOE_DEV, 0)
    own_rank = lax.dynamic_slice_in_dim(
        rank_in.reshape(-1, top_count), own_block * MOE_DEV, MOE_DEV, 0
    )
    own_weight = lax.dynamic_slice_in_dim(route_weight, own_block * MOE_DEV, MOE_DEV, 0)
    picked = arrived_sums.reshape(-1, width)[own_entries * capacity + own_rank]
    moe_out = (
        jnp.sum(own_weight[..., None] * picked, 1) + shared_total.reshape(MOE_DEV, width)
    ).astype(jnp.bfloat16)
    return (mixed, moe_out)


def solution(mesh):
    in_specs = (
        P("ep", None),
        P("ep", None),
        P("ep", None),
        P(),
        P(),
        P(None, "tp"),
        P(None, "tp"),
        P(None, "tp"),
        P("ep", None),
        P(),
        P("ep", None),
        P("ep", None),
        P("ep", None, "tp"),
        P("ep", None, "tp"),
        P("ep", "tp", None),
        P(None, "tp"),
        P(None, "tp"),
        P("tp", None),
    )
    out_specs = (P("ep", "tp"), P(("ep", "tp"), None))
    return jax.shard_map(body, mesh=mesh, in_specs=in_specs, out_specs=out_specs, check_vma=False)
```

profile of v0, /device:TPU:0, one launch (start us, length us, event | category | flops | bytes accessed | tf_op | source)
XLA Modules:
  0.0 239.6 jit_solution(11745356198436479961)
XLA Ops:
  8.0 1.0 copy.32
  9.0 0.7 broadcast_multiply_fusion
  9.9 1.4 fusion.80
  11.8 2.4 %scatter_custom_fusion = s32[768]{0:T(1024)S(1)} fusion(s32[512]{0:T(512)S(1)} %bitcast.88, s32[512]{0:T(512)S(1)} %add_select_fusion, s32[]{:T(128)} %constant.90.clone.1), kind=kCustom, calls=%fused_computation.110 | custom fusion | bytes 3076 | tf_op jit(solution)/shard_map/scatter | solution.py:193
  14.3 1.4 convert_reduce_fusion
  16.3 1.6 fusion.40
  17.9 4.3 %gather_fusion = bf16[768,2048]{1,0:T(8,128)(2,1)} fusion(bf16[256,2048]{1,0:T(8,128)(2,1)S(1)} %fusion.40, s32[1024]{0:T(1024)S(1)} %pad_clamp_fusion.1), kind=kCustom, calls=%fused_computation | custom fusion | bytes 6294528 | tf_op jit(solution)/shard_map/gather | solution.py:196
  22.2 3.8 %broadcast_select_fusion = bf16[4,1,8,24,2048]{4,3,2,1,0:T(8,128)(2,1)} fusion(bf16[4,1,8,24,2048]{4,3,2,1,0:T(8,128)(2,1)} %bitcast.82, pred[4,8,24]{2,1,0:T(8,128)(4,1)S(1)} %broadcast_in_dim.44), kind=kLoop, calls=%fused_computation.38 | loop fusion | flops 1572864 | bytes 6292224 | tf_op jit(solution)/shard_map/jit(_where)/select_n | solution.py:195
  26.0 5.3 %all-to-all-start = ((bf16[4,1,8,24,2048]{4,3,2,1,0:T(8,128)(2,1)}), bf16[4,1,8,24,2048]{4,3,2,1,0:T(8,128)(2,1)}, u32[]{:S(2)}, u32[]{:S(2)}) async-start(bf16[4,1,8,24,2048]{4,3,2,1,0:T(8,128)(2,1)} %broadcast_select_fusion), calls=%async_computation | async-start | bytes 6291456 | tf_op jit(solution)/shard_map/all_to_all | solution.py:199
  31.4 1.3 fusion.52
  32.6 2.0 fusion.54
  34.8 39.4 %all-to-all-done = bf16[4,1,8,24,2048]{4,3,2,1,0:T(8,128)(2,1)} async-done(((bf16[4,1,8,24,2048]{4,3,2,1,0:T(8,128)(2,1)}), bf16[4,1,8,24,2048]{4,3,2,1,0:T(8,128)(2,1)}, u32[]{:S(2)}, u32[]{:S(2)}) %all-to-all-start) | async-done | bytes 3145760 | tf_op jit(solution)/shard_map/all_to_all | solution.py:199
  74.1 5.6 %fusion.47 = f32[768,512]{1,0:T(8,128)} fusion(bf16[768,2048]{1,0:T(8,128)(2,1)} %bitcast.12, bf16[1,2048,512]{2,1,0:T(8,128)(2,1)} %param.34), kind=kOutput, calls=%fused_computation.55 | convolution fusion | flops 1610612736 | bytes 6815744 | tf_op jit(solution)/shard_map/dot_general | solution.py:202
  79.7 8.2 %convolution_convert_fusion.1 = bf16[768,2048]{1,0:T(8,128)(2,1)} fusion(bf16[1,512,2048]{2,1,0:T(8,128)(2,1)S(1)} %copy-done, f32[768,512]{1,0:T(8,128)} %fusion.47, bf16[768,2048]{1,0:T(8,128)(2,1)} %bitcast.12, bf16[1,2048,512]{2,1,0:T(8,128)(2,1)} %param.35), kind=kOutput, calls=%fused_computation.37 | convolution fusion | flops 3225157632 | bytes 12058624 | tf_op jit(solution)/shard_map/dot_general | solution.py:206
  88.0 1.7 fusion.81
  89.7 3.9 %convolution_convert_fusion.2 = bf16[256,2048]{1,0:T(8,128)(2,1)} fusion(bf16[256,2048]{1,0:T(8,128)(2,1)} %param.39, bf16[256,2048]{1,0:T(8,128)(2,1)S(1)} %fusion.40, bf16[2048,256]{1,0:T(8,128)(2,1)} %param.38, f32[256,256]{1,0:T(8,128)S(1)} %fusion.81), kind=kOutput, calls=%fused_computation.43 | convolution fusion | flops 537788416 | bytes 4456448 | tf_op jit(solution)/shard_map/dot_general | solution.py:213
  93.7 0.9 convert_element_type.97
  94.6 1.5 fusion.41
  96.1 1.5 fusion.55
  97.7 0.9 copy-done.4
  99.0 9.5 %all_gather.10 = bf16[4096,32]{0,1:T(8,128)(2,1)S(1)} all-gather(bf16[1024,32]{0,1:T(8,128)(2,1)S(1)} %pad_maximum_fusion.1), channel_id=1, replica_groups=mesh['ep'=4,'tp'=8] {'ep'}, dimensions={0}, use_global_device_ids=true | all-gather | bytes 327680 | tf_op jit(solution)/shard_map/all_gather | solution.py:147
  108.4 1.0 subtract_convert_fusion
  109.5 0.5 iota.29
  110.1 0.6 broadcast_in_dim.40
  110.7 16.7 %while.15 = (s32[]{:T(128)}, f32[1024,2]{0,1:T(2,128)}, f32[1024,2]{0,1:T(2,128)S(1)}, f32[1024,2,64]{0,2,1:T(8,128)S(1)}, s32[4]{0:T(128)}, /*index=5*/s32[]{:T...) while((s32[]{:T(128)}, f32[1024,2]{0,1:T(2,128)}, ...), condition=%wide.region_7.8_spmd.clone, body=%wide.region_2.7_spmd.clone.sunk | while | flops 824059904 | bytes 47456656 | solution.py:164
  110.7 1.3 dynamic_slice.35
  112.6 8.7 %conditional.3 = ((f32[1024,2]{0,1:T(2,128)}, f32[1024,2]{0,1:T(2,128)S(1)}, f32[1024,2,64]{0,2,1:T(8,128)S(1)})) conditional(s32[]{:T(128)} %convert_element_type.190, (f32[1024,2]{0,1:T(2,128)}, f32[1024,2]{0,1:T(2,128)S(1)}, f32[1024,2,64]{0,2,1:T(8,128)S(1)}) %tuple.45, (s32[]{:T(128)}, s32[]{:T(128)}, bf16[4096,256]{1,0:T(8,128)(2,1)}, ...), branch_computations={%region_3.3_spmd, %region_4.6_spmd} | conditional | flops 824059904 | bytes 47452312 | solution.py:162
  113.3 1.4 convolution_convert_fusion
  114.7 1.3 fusion.26
  116.0 0.7 broadcast_compare_fusion
  116.7 2.0 fusion.79
  118.7 1.1 fusion.5
  119.9 1.5 fusion.21
  121.4 1.3 dynamic_slice.35
  123.4 1.3 dynamic_slice.35
  125.4 1.3 dynamic_slice.35
  127.4 0.8 divide_convert_fusion
  128.3 1.2 dynamic-slice
  129.6 35.7 %all-reduce.3.cloned.1.call-done = bf16[4,1,8,24,2048]{4,3,2,0,1:T(8,128)(2,1)} async-done(((bf16[4,1,8,24,2048]{4,3,2,0,1:T(8,128)(2,1)}), bf16[4,1,8,24,2048]{4,3,2,0,1:T(8,128)(2,1)}) %all-reduce.3.cloned.1.call-update) | async-done | bytes 3145744
  165.3 2.4 %dynamic-slice_bitcast_fusion = bf16[4,1,1,24,2048]{4,3,2,1,0:T(8,128)(2,1)} fusion(bf16[4,1,8,24,2048]{4,3,2,0,1:T(8,128)(2,1)} %all-reduce.3.cloned.1.call-done, u32[]{:T(128)} %bitcast.27), kind=kLoop, calls=%fused_computation.76 | loop fusion | bytes 786436 | tf_op jit(solution)/shard_map/reduce_scatter | solution.py:217
  167.7 3.6 %all-to-all-start.1 = ((bf16[4,1,1,24,2048]{4,3,2,1,0:T(8,128)(2,1)}), bf16[4,1,1,24,2048]{4,3,2,1,0:T(8,128)(2,1)S(1)}, u32[]{:S(2)}, u32[]{:S(2)}) async-start(bf16[4,1,1,24,2048]{4,3,2,1,0:T(8,128)(2,1)} %dynamic-slice_bitcast_fusion), calls=%async_computation.1 | async-start | bytes 786432 | tf_op jit(solution)/shard_map/all_to_all | solution.py:232
  171.6 5.6 %all-to-all-done.1 = bf16[4,1,1,24,2048]{4,3,2,1,0:T(8,128)(2,1)S(1)} async-done(((bf16[4,1,1,24,2048]{4,3,2,1,0:T(8,128)(2,1)}), bf16[4,1,1,24,2048]{4,3,2,1,0:T(8,128)(2,1)S(1)}, u32[]{:S(2)}, u32[]{:S(2)}) %all-to-all-start.1) | async-done | bytes 393248 | tf_op jit(solution)/shard_map/all_to_all | solution.py:232
  177.3 0.8 gather_fusion.1
  178.4 0.7 multiply_reduce_fusion
  179.1 20.7 %reduce-scatter.3.cloned.1.call-done = bf16[1,1,1,32,2048]{4,3,2,1,0:T(8,128)(2,1)} async-done(((bf16[1,1,8,32,2048]{4,3,2,1,0:T(8,128)(2,1)}), bf16[1,1,1,32,2048]{4,3,2,1,0:T(8,128)(2,1)}) %reduce-scatter.3.cloned.1.call-update) | async-done | bytes 131088 | tf_op jit(solution)/shard_map/reduce_scatter | solution.py:223
  199.9 1.6 fusion.62
  201.4 27.3 %all-gather.5.cloned.1.call-done = bf16[1024,1024]{0,1:T(8,128)(2,1)} async-done(((bf16[1024,128]{0,1:T(8,128)(2,1)}), bf16[1024,1024]{0,1:T(8,128)(2,1)}) %all-gather.5.cloned.1.call-update) | async-done | bytes 2097168 | tf_op jit(solution)/shard_map/all_gather | solution.py:172
  228.8 3.2 %convolution_convert_fusion.3 = bf16[1024,256]{1,0:T(8,128)(2,1)} fusion(bf16[1024,1024]{0,1:T(8,128)(2,1)} %all-gather.5.cloned.1.call-done, bf16[1024,256]{1,0:T(8,128)(2,1)} %param.29), kind=kOutput, calls=%fused_computation.60 | convolution fusion | flops 537133056 | bytes 3145728 | tf_op jit(solution)/shard_map/dot_general | solution.py:171
  (74 shorter events, 2.9 us)
Async XLA Ops:
  8.0 71.7 %copy-start = (bf16[1,512,2048]{2,1,0:T(8,128)(2,1)S(1)}, bf16[1,512,2048]{2,1,0:T(8,128)(2,1)}, u32[]{:S(2)}) copy-start(bf16[1,512,2048]{2,1,0:T(8,128)(2,1)} %param.36) | copy-start | bytes 6291460
  8.0 7.7 %copy-start.1 = (bf16[256,2048]{1,0:T(8,128)(2,1)S(1)}, bf16[256,2048]{1,0:T(8,128)(2,1)}, u32[]{:S(2)}) copy-start(bf16[256,2048]{1,0:T(8,128)(2,1)} %param.30) | copy-start | bytes 3145732
  8.0 8.3 %copy-start.7 = (f32[2048]{0:T(1024)S(1)}, f32[2048]{0:T(1024)}, u32[]{:S(2)}) copy-start(f32[2048]{0:T(1024)} %param.31) | copy-start | bytes 24580
  26.0 6.6 %copy-start.8 = (f32[256]{0:T(256)S(1)}, f32[256]{0:T(256)}, u32[]{:S(2)}) copy-start(f32[256]{0:T(256)} %param.26) | copy-start | bytes 3076
  26.0 48.1 %all-to-all-start = ((bf16[4,1,8,24,2048]{4,3,2,1,0:T(8,128)(2,1)}), bf16[4,1,8,24,2048]{4,3,2,1,0:T(8,128)(2,1)}, u32[]{:S(2)}, u32[]{:S(2)}) async-start(bf16[4,1,8,24,2048]{4,3,2,1,0:T(8,128)(2,1)} %broadcast_select_fusion), calls=%async_computation | async-start | bytes 6291456 | tf_op jit(solution)/shard_map/all_to_all | solution.py:199
  31.4 78.1 %all-gather.3.cloned.1.call-start = ((), (), s32[]{:S(2)}) async-start(), calls=%async_computation.3 | async-start | bytes 2621440 | tf_op jit(solution)/shard_map/all_gather | solution.py:146
  34.7 130.6 %all-reduce.3.cloned.1.call-start = ((), (), s32[]{:S(2)}) async-start(), calls=%async_computation.6 | async-start | bytes 6291456
  88.0 111.9 %reduce-scatter.3.cloned.1.call-start = ((), (), s32[]{:S(2)}) async-start(), calls=%async_computation.5 | async-start | bytes 1179648 | tf_op jit(solution)/shard_map/reduce_scatter | solution.py:223
  93.6 2.5 %copy-start.3 = (bf16[1024,512]{1,0:T(8,128)(2,1)S(1)}, bf16[1024,512]{1,0:T(8,128)(2,1)}, u32[]{:S(2)}) copy-start(bf16[1024,512]{1,0:T(8,128)(2,1)} %param.22) | copy-start | bytes 3145732
  93.6 2.5 %copy-start.10 = (f32[512]{0:T(512)S(1)}, f32[512]{0:T(512)}, u32[]{:S(2)}) copy-start(f32[512]{0:T(512)} %param.25) | copy-start | bytes 6148
  93.6 135.2 %all-gather.5.cloned.1.call-start = ((), (), s32[]{:S(2)}) async-start(), calls=%async_computation.4 | async-start | bytes 2359296 | tf_op jit(solution)/shard_map/all_gather | solution.py:172
  97.7 0.9 copy-start.4
  97.7 13.0 %copy-start.2 = (bf16[256,256]{1,0:T(8,128)(2,1)S(1)}, bf16[256,256]{1,0:T(8,128)(2,1)}, u32[]{:S(2)}) copy-start(bf16[256,256]{1,0:T(8,128)(2,1)} %param.28) | copy-start | bytes 393220
  118.7 1.1 copy-start.5
  119.8 1.5 copy-start.6
  127.4 44.1 %copy-start.9 = (f32[256,2]{0,1:T(2,128)S(1)}, f32[256,2]{0,1:T(2,128)}, u32[]{:S(2)}) copy-start(f32[256,2]{0,1:T(2,128)} %param.33) | copy-start | bytes 6148
  167.7 9.5 %all-to-all-start.1 = ((bf16[4,1,1,24,2048]{4,3,2,1,0:T(8,128)(2,1)}), bf16[4,1,1,24,2048]{4,3,2,1,0:T(8,128)(2,1)S(1)}, u32[]{:S(2)}, u32[]{:S(2)}) async-start(bf16[4,1,1,24,2048]{4,3,2,1,0:T(8,128)(2,1)} %dynamic-slice_bitcast_fusion), calls=%async_computation.1 | async-start | bytes 786432 | tf_op jit(solution)/shard_map/all_to_all | solution.py:232
Sparse Core Ops, SparseCore 0:
  34.8 58.6 all-gather.2
Sparse Core Ops, SparseCore 1:
  88.0 77.2 all-reduce.2
  167.4 32.4 reduce-scatter.2
  201.3 27.4 all-gather.4
where the time goes:
time: 241 us; the launch traced here: 240 us
  waiting for transfers between devices  129 us (54%)
  matrix products  30.3 us (13%)
  other arithmetic  21.5 us (9%)
  local copies, waits for them, and re-layouts  21 us (9%)
  between operations  16 us (7%)
  blocking collectives  9.47 us (4%)
  starting transfers between devices  9.1 us (4%)
  loops' own time  3.42 us (1%)
    all_to_all x1, waiting for transfers between devices, body(): lax.all_to_all(outgoing, 'ep', split_axis=0, concat_axis=0, tiled=True)  39.4 us
    unnamed x5, waiting for transfers between devices  35.8 us
    all_gather x1, waiting for transfers between devices, body(): lax.all_gather(heads_out, 'tp', axis=1, tiled=True)  27.3 us
    reduce_scatter x1, waiting for transfers between devices, body(): lax.psum_scatter(shared_part.astype(jnp.float32).reshape(1, 1, tp_count,...  20.7 us
    all_gather x1, blocking collectives, body(): rotated_piece = lax.all_gather(key_rotated, 'ep', axis=0, tiled=True)  9.47 us
    dot_general x1, matrix products, body(): output = jnp.dot(hidden, expert_down[0], preferred_element_type=jnp.float32)  8.25 us
    all_to_all x1, waiting for transfers between devices, body(): lax.all_to_all(slot_total.astype(jnp.bfloat16), 'ep', split_axis=0, conca...  5.58 us
    dot_general x1, matrix products, body(): jnp.dot(inputs, expert_gate[0], preferred_element_type=jnp.float32)  5.57 us
  transfers between devices with their start and end apart: 6, of which 5 were waited for; matrix products, arithmetic and copies ran while one was open for 21% of the time, Pallas kernels for 0%

commit v1 on v0

--- a/solution.py
+++ b/solution.py
@@ -11,6 +11,27 @@
 layer_eps = 1e-05
 rotary_base = 10000.0
 floor_value = -1e30
+
+
+def gather_around(shard, axis, dim):
+    size, mine, rows = (lax.axis_size(axis), lax.axis_index(axis), shard.shape[dim])
+    right = [(i, (i + 1) % size) for i in range(size)]
+    backward = [(i, (i - 1) % size) for i in range(size)]
+    filled = jnp.zeros((*shard.shape[:dim], size * rows, *shard.shape[dim + 1 :]), shard.dtype)
+    filled = lax.dynamic_update_slice_in_dim(filled, shard, mine * rows, axis=dim)
+    from_left = from_right = shard
+    halfway = size // 2
+    for step in range(1, halfway + 1):
+        from_left = lax.ppermute(from_left, axis, right)
+        filled = lax.dynamic_update_slice_in_dim(
+            filled, from_left, (mine - step) % size * rows, axis=dim
+        )
+        if step < size - halfway:
+            from_right = lax.ppermute(from_right, axis, backward)
+            filled = lax.dynamic_update_slice_in_dim(
+                filled, from_right, (mine + step) % size * rows, axis=dim
+            )
+    return filled
 
 
 def rms_scale(values, gain):
@@ -168,11 +189,7 @@
         .astype(jnp.bfloat16)
         .reshape(row_count, heads_local * VDIM)
     )
-    mixed = jnp.dot(
-        lax.all_gather(heads_out, "tp", axis=1, tiled=True),
-        w_output,
-        preferred_element_type=jnp.float32,
-    )
+    mixed = jnp.dot(gather_around(heads_out, "tp", 1), w_output, preferred_element_type=jnp.float32)
     mixed = mixed.astype(jnp.bfloat16)
     width = moe_input.shape[1]
     top_count = routes.shape[1]

time: 241 us -> 228 us (0.946)
  waiting for transfers between devices: 129 us -> 83.5 us
  starting transfers between devices: 9.1 us -> 28.2 us
  local copies, waits for them, and re-layouts: 21 us -> 31.7 us
    all_gather x1 -> x0, waiting for transfers between devices: 27.3 us -> none  [body(): lax.all_gather(heads_out, 'tp', axis=1, tiled=True)]
    unnamed x5 -> x4, waiting for transfers between devices: 35.8 us -> 14.1 us
    ppermute x0 -> x7, waiting for transfers between devices: none -> 18.5 us  [the longest x3 15.9 us: gather_around(): from_right = lax.ppermute(from_right, axis, backward)]
    ppermute x0 -> x7, starting transfers between devices: none -> 11.1 us  [the longest x3 11 us: gather_around(): from_right = lax.ppermute(from_right, axis, backward)]
    all_to_all x1, starting transfers between devices: 3.65 us -> 11.7 us  [body(): lax.all_to_all(slot_total.astype(jnp.bfloat16), 'ep', split_axis=0, conca...]
    dynamic_update_slice x0 -> x8, local copies, waits for them, and re-layouts: none -> 6.73 us  [the longest x4 3.85 us: gather_around(): lax.dynamic_update_slice_in_dim(filled, from_left, (mine - step) % size *...]
    all_to_all x1, waiting for transfers between devices: 39.4 us -> 34.2 us  [body(): lax.all_to_all(outgoing, 'ep', split_axis=0, concat_axis=0, tiled=True)]
    all_to_all x1, waiting for transfers between devices: 5.58 us -> 0.46 us  [body(): lax.all_to_all(slot_total.astype(jnp.bfloat16), 'ep', split_axis=0, conca...]
  transfers between devices with their start and end apart: 6 -> 12, of which waited for: 5 -> 7; matrix products, arithmetic and copies ran while one was open for 21% -> 28% of each run, Pallas kernels for 0% -> 0%
where the time goes in v1:
time: 228 us; the launch traced here: 227 us
  waiting for transfers between devices  83.5 us (37%)
  local copies, waits for them, and re-layouts  31.7 us (14%)
  matrix products  31.2 us (14%)
  starting transfers between devices  28.2 us (12%)
  other arithmetic  22.7 us (10%)
  between operations  16 us (7%)
  blocking collectives  9.97 us (4%)
  loops' own time  3.35 us (1%)
    all_to_all x1, waiting for transfers between devices, body(): lax.all_to_all(outgoing, 'ep', split_axis=0, concat_axis=0, tiled=True)  34.2 us
    reduce_scatter x1, waiting for transfers between devices, body(): lax.psum_scatter(shared_part.astype(jnp.float32).reshape(1, 1, tp_count,...  16.2 us
    ppermute x3, waiting for transfers between devices, gather_around(): from_right = lax.ppermute(from_right, axis, backward)  15.9 us
    unnamed x4, waiting for transfers between devices  14.1 us
    all_to_all x1, starting transfers between devices, body(): lax.all_to_all(slot_total.astype(jnp.bfloat16), 'ep', split_axis=0, conca...  11.7 us
    ppermute x3, starting transfers between devices, gather_around(): from_right = lax.ppermute(from_right, axis, backward)  11 us
    all_gather x1, blocking collectives, body(): rotated_piece = lax.all_gather(key_rotated, 'ep', axis=0, tiled=True)  9.97 us
    dot_general x1, matrix products, body(): output = jnp.dot(hidden, expert_down[0], preferred_element_type=jnp.float32)  8.24 us
  transfers between devices with their start and end apart: 12, of which 7 were waited for; matrix products, arithmetic and copies ran while one was open for 28% of the time, Pallas kernels for 0%

profile of v1, /device:TPU:0, one launch (start us, length us, event | category | flops | bytes accessed | tf_op | source)
XLA Modules:
  0.0 226.6 jit_solution(6545257784724455926)
XLA Ops:
  8.0 1.0 copy.32
  9.9 1.4 fusion.80
  11.9 2.4 %scatter_custom_fusion = s32[768]{0:T(1024)S(1)} fusion(s32[512]{0:T(512)S(1)} %bitcast.90, s32[512]{0:T(512)S(1)} %add_select_fusion, s32[]{:T(128)} %constant.133.clone.1), kind=kCustom, calls=%fused_computation.119 | custom fusion | bytes 3076 | tf_op jit(solution)/shard_map/scatter | solution.py:210
  14.3 1.4 convert_reduce_fusion
  16.3 1.6 fusion.40
  18.0 4.3 %gather_fusion = bf16[768,2048]{1,0:T(8,128)(2,1)} fusion(bf16[256,2048]{1,0:T(8,128)(2,1)S(1)} %fusion.40, s32[1024]{0:T(1024)S(1)} %pad_clamp_fusion.1), kind=kCustom, calls=%fused_computation | custom fusion | bytes 6294528 | tf_op jit(solution)/shard_map/gather | solution.py:213
  22.3 3.8 %broadcast_select_fusion = bf16[4,1,8,24,2048]{4,3,2,1,0:T(8,128)(2,1)} fusion(bf16[4,1,8,24,2048]{4,3,2,1,0:T(8,128)(2,1)} %bitcast.82, pred[4,8,24]{2,1,0:T(8,128)(4,1)S(1)} %broadcast_in_dim.51), kind=kLoop, calls=%fused_computation.38 | loop fusion | flops 1572864 | bytes 6292224 | tf_op jit(solution)/shard_map/jit(_where)/select_n | solution.py:212
  26.1 5.3 %all-to-all-start = ((bf16[4,1,8,24,2048]{4,3,2,1,0:T(8,128)(2,1)}), bf16[4,1,8,24,2048]{4,3,2,1,0:T(8,128)(2,1)}, u32[]{:S(2)}, u32[]{:S(2)}) async-start(bf16[4,1,8,24,2048]{4,3,2,1,0:T(8,128)(2,1)} %broadcast_select_fusion), calls=%async_computation | async-start | bytes 6291456 | tf_op jit(solution)/shard_map/all_to_all | solution.py:216
  31.4 1.3 fusion.52
  32.8 2.0 fusion.54
  35.0 1.5 fusion.41
  36.5 1.8 fusion.55
  38.3 0.9 copy-done.6
  40.0 34.2 %all-to-all-done = bf16[4,1,8,24,2048]{4,3,2,1,0:T(8,128)(2,1)} async-done(((bf16[4,1,8,24,2048]{4,3,2,1,0:T(8,128)(2,1)}), bf16[4,1,8,24,2048]{4,3,2,1,0:T(8,128)(2,1)}, u32[]{:S(2)}, u32[]{:S(2)}) %all-to-all-start) | async-done | bytes 3145760 | tf_op jit(solution)/shard_map/all_to_all | solution.py:216
  74.2 5.5 %fusion.47 = f32[768,512]{1,0:T(8,128)} fusion(bf16[768,2048]{1,0:T(8,128)(2,1)} %bitcast.12, bf16[1,2048,512]{2,1,0:T(8,128)(2,1)} %param.34), kind=kOutput, calls=%fused_computation.55 | convolution fusion | flops 1610612736 | bytes 6815744 | tf_op jit(solution)/shard_map/dot_general | solution.py:219
  79.7 8.2 %convolution_convert_fusion.1 = bf16[768,2048]{1,0:T(8,128)(2,1)} fusion(bf16[1,512,2048]{2,1,0:T(8,128)(2,1)S(1)} %copy-done, f32[768,512]{1,0:T(8,128)} %fusion.47, bf16[768,2048]{1,0:T(8,128)(2,1)} %bitcast.12, bf16[1,2048,512]{2,1,0:T(8,128)(2,1)} %param.35), kind=kOutput, calls=%fused_computation.37 | convolution fusion | flops 3225157632 | bytes 12058624 | tf_op jit(solution)/shard_map/dot_general | solution.py:223
  88.4 10.0 %all_gather.7 = bf16[4096,32]{0,1:T(8,128)(2,1)} all-gather(bf16[1024,32]{0,1:T(8,128)(2,1)S(1)} %pad_maximum_fusion.1), channel_id=1, replica_groups=mesh['ep'=4,'tp'=8] {'ep'}, dimensions={0}, use_global_device_ids=true | all-gather | bytes 327680 | tf_op jit(solution)/shard_map/all_gather | solution.py:168
  98.3 1.0 subtract_convert_fusion
  99.3 1.0 pad_maximum_fusion
  100.3 1.1 fusion.81
  102.1 0.8 broadcast_in_dim.45
  103.5 18.5 %while.15 = (s32[]{:T(128)}, f32[1024,2]{0,1:T(2,128)}, f32[1024,2]{0,1:T(2,128)S(1)}, f32[1024,2,64]{0,2,1:T(8,128)}, s32[4]{0:T(128)}, /*index=5*/s32[]{:T(128...) while((s32[]{:T(128)}, f32[1024,2]{0,1:T(2,128)}, ...), condition=%wide.region_7.8_spmd.clone, body=%wide.region_2.7_spmd.clone.sunk | while | flops 824059904 | bytes 51651016 | solution.py:185
  103.5 1.3 dynamic_slice.35
  105.5 10.6 %conditional.3 = ((f32[1024,2]{0,1:T(2,128)}, f32[1024,2]{0,1:T(2,128)S(1)}, f32[1024,2,64]{0,2,1:T(8,128)})) conditional(s32[]{:T(128)} %convert_element_type.190, (f32[1024,2]{0,1:T(2,128)}, f32[1024,2]{0,1:T(2,128)S(1)}, f32[1024,2,64]{0,2,1:T(8,128)}) %tuple.45, (s32[]{:T(128)}, s32[]{:T(128)}, bf16[4096,256]{1,0:T(8,128)(2,1)}, ...), branch_computations={%region_3.3_spmd, %region_4.6_spmd} | conditional | flops 824059904 | bytes 51646672 | solution.py:183
  106.1 1.4 convolution_convert_fusion
  107.5 1.3 fusion.26
  109.5 3.0 %fusion.79 = (f32[2,1024]{1,0:T(2,128)S(1)}, f32[2,1024,1024]{1,2,0:T(8,128)S(1)}) fusion(bf16[1024,2,96]{0,2,1:T(8,128)(2,1)S(1)} %get-tuple-element.73, bf16[4096,32]{0,1:T(8,128)(2,1)} %get-tuple-element.74, s32[]{:T(128)S(6)} %select_n.76, f32[2,1024,1024]{2,1,0:T(8,128)S(1)} %fusion.26, pred[1024,1024]{0,1:T(8,128)(4,1)S(1)} %broadcast_compare_fusion), kind=kOutput, calls=%fused_computation.128 | convolution fusion | flops 142604288 | bytes 18030596 | tf_op jit(solution)/shard_map/while/body/eval_jaxpr/cond/branch_1_fun/qhd,kd->hqk/dot_general | solution.py:82
  112.5 1.1 fusion.5
  113.7 1.5 fusion.21
  116.0 1.3 dynamic_slice.35
  118.0 1.3 dynamic_slice.35
  120.0 1.3 dynamic_slice.35
  122.0 1.1 divide_convert_fusion
  123.2 4.0 %convolution_convert_fusion.2 = bf16[256,2048]{1,0:T(8,128)(2,1)} fusion(bf16[256,2048]{1,0:T(8,128)(2,1)} %param.39, bf16[256,2048]{1,0:T(8,128)(2,1)S(1)} %fusion.40, bf16[2048,256]{1,0:T(8,128)(2,1)} %param.38, f32[256,256]{1,0:T(8,128)} %fusion.81), kind=kOutput, calls=%fused_computation.43 | convolution fusion | flops 537788416 | bytes 4456448 | tf_op jit(solution)/shard_map/dot_general | solution.py:230
  127.4 3.6 %collective-permute-start.1 = (bf16[1024,128]{0,1:T(8,128)(2,1)S(1)}, bf16[1024,128]{0,1:T(8,128)(2,1)S(1)}, u32[]{:S(2)}, u32[]{:S(2)}) collective-permute-start(bf16[1024,128]{0,1:T(8,128)(2,1)S(1)} %bitcast.85), channel_id=1, source_target_pairs={{0,7},{1,0},{2,1},{3,2},{4,3},{5,4},{6,5},{7,6},{8,15},{9,8},{10,9... | collective-permute-start | bytes 786440 | tf_op jit(solution)/shard_map/ppermute | solution.py:30
  133.3 8.2 %collective-permute-done.1 = bf16[1024,128]{0,1:T(8,128)(2,1)S(1)} collective-permute-done((bf16[1024,128]{0,1:T(8,128)(2,1)S(1)}, bf16[1024,128]{0,1:T(8,128)(2,1)S(1)}, u32[]{:S(2)}, u32[]{:S(2)}) %collective-permute-start.1) | collective-permute-done | bytes 262176 | tf_op jit(solution)/shard_map/ppermute | solution.py:30
  141.5 3.7 %collective-permute-start.3 = (bf16[1024,128]{0,1:T(8,128)(2,1)S(1)}, bf16[1024,128]{0,1:T(8,128)(2,1)S(1)}, u32[]{:S(2)}, u32[]{:S(2)}) collective-permute-start(bf16[1024,128]{0,1:T(8,128)(2,1)S(1)} %collective-permute-done.1), channel_id=1, source_target_pairs={{0,7},{1,0},{2,1},{3,2},{4,3},{5,4},{6,5},{7,6},{8,15},{9,8},{10,9... | collective-permute-start | bytes 786440 | tf_op jit(solution)/shard_map/ppermute | solution.py:30
  145.2 1.6 broadcast_in_dim.42
  147.5 1.7 constant_dynamic-update-slice_fusion.6
  149.9 7.7 %collective-permute-done.3 = bf16[1024,128]{0,1:T(8,128)(2,1)S(1)} collective-permute-done((bf16[1024,128]{0,1:T(8,128)(2,1)S(1)}, bf16[1024,128]{0,1:T(8,128)(2,1)S(1)}, u32[]{:S(2)}, u32[]{:S(2)}) %collective-permute-start.3) | collective-permute-done | bytes 262176 | tf_op jit(solution)/shard_map/ppermute | solution.py:30
  157.6 3.7 %collective-permute-start.5 = (bf16[1024,128]{0,1:T(8,128)(2,1)S(1)}, bf16[1024,128]{0,1:T(8,128)(2,1)S(1)}, u32[]{:S(2)}, u32[]{:S(2)}) collective-permute-start(bf16[1024,128]{0,1:T(8,128)(2,1)S(1)} %collective-permute-done.3), channel_id=1, source_target_pairs={{0,7},{1,0},{2,1},{3,2},{4,3},{5,4},{6,5},{7,6},{8,15},{9,8},{10,9... | collective-permute-start | bytes 786440 | tf_op jit(solution)/shard_map/ppermute | solution.py:30
  162.8 2.6 %collective-permute-done.4 = bf16[1024,128]{0,1:T(8,128)(2,1)S(1)} collective-permute-done((bf16[1024,128]{0,1:T(8,128)(2,1)S(1)}, bf16[1024,128]{0,1:T(8,128)(2,1)S(1)}, u32[]{:S(2)}, u32[]{:S(2)}) %collective-permute-start.4) | collective-permute-done | bytes 262176 | tf_op jit(solution)/shard_map/ppermute | solution.py:25
  165.4 14.1 %all-reduce.3.cloned.1.call-done = bf16[4,1,8,24,2048]{4,3,2,0,1:T(8,128)(2,1)} async-done(((bf16[4,1,8,24,2048]{4,3,2,0,1:T(8,128)(2,1)}), bf16[4,1,8,24,2048]{4,3,2,0,1:T(8,128)(2,1)}) %all-reduce.3.cloned.1.call-update) | async-done | bytes 3145744
  179.5 2.4 %dynamic-slice_bitcast_fusion = bf16[4,1,1,24,2048]{4,3,2,1,0:T(8,128)(2,1)} fusion(bf16[4,1,8,24,2048]{4,3,2,0,1:T(8,128)(2,1)} %all-reduce.3.cloned.1.call-done, u32[]{:T(128)} %bitcast.27), kind=kLoop, calls=%fused_computation.76 | loop fusion | bytes 786436 | tf_op jit(solution)/shard_map/reduce_scatter | solution.py:234
  181.9 11.7 %all-to-all-start.1 = ((bf16[4,1,1,24,2048]{4,3,2,1,0:T(8,128)(2,1)}), bf16[4,1,1,24,2048]{4,3,2,1,0:T(8,128)(2,1)S(1)}, u32[]{:S(2)}, u32[]{:S(2)}) async-start(bf16[4,1,1,24,2048]{4,3,2,1,0:T(8,128)(2,1)} %dynamic-slice_bitcast_fusion), calls=%async_computation.1 | async-start | bytes 786432 | tf_op jit(solution)/shard_map/all_to_all | solution.py:249
  195.7 3.3 %convolution_convert_fusion.3 = bf16[1024,256]{1,0:T(8,128)(2,1)} fusion(bf16[1024,1024]{0,1:T(8,128)(2,1)} %constant_dynamic-update-slice_fusion, bf16[1024,256]{1,0:T(8,128)(2,1)} %param.29), kind=kOutput, calls=%fused_computation.60 | convolution fusion | flops 537133056 | bytes 3145728 | tf_op jit(solution)/shard_map/dot_general | solution.py:192
  201.4 16.2 %reduce-scatter.3.cloned.1.call-done = bf16[1,1,1,32,2048]{4,3,2,1,0:T(8,128)(2,1)} async-done(((bf16[1,1,8,32,2048]{4,3,2,1,0:T(8,128)(2,1)}), bf16[1,1,1,32,2048]{4,3,2,1,0:T(8,128)(2,1)}) %reduce-scatter.3.cloned.1.call-update) | async-done | bytes 131088 | tf_op jit(solution)/shard_map/reduce_scatter | solution.py:240
  217.6 1.6 fusion.62
  (106 shorter events, 15.9 us)
Async XLA Ops:
  8.0 71.7 %copy-start = (bf16[1,512,2048]{2,1,0:T(8,128)(2,1)S(1)}, bf16[1,512,2048]{2,1,0:T(8,128)(2,1)}, u32[]{:S(2)}) copy-start(bf16[1,512,2048]{2,1,0:T(8,128)(2,1)} %param.36) | copy-start | bytes 6291460
  8.0 7.8 %copy-start.3 = (bf16[256,2048]{1,0:T(8,128)(2,1)S(1)}, bf16[256,2048]{1,0:T(8,128)(2,1)}, u32[]{:S(2)}) copy-start(bf16[256,2048]{1,0:T(8,128)(2,1)} %param.30) | copy-start | bytes 3145732
  8.0 8.3 %copy-start.11 = (f32[2048]{0:T(1024)S(1)}, f32[2048]{0:T(1024)}, u32[]{:S(2)}) copy-start(f32[2048]{0:T(1024)} %param.31) | copy-start | bytes 24580
  9.0 9.0 %copy-start.5 = (s32[256,2]{1,0:T(8,128)}, s32[256,2]{1,0:T(8,128)S(1)}, u32[]{:S(2)}) copy-start(s32[256,2]{1,0:T(8,128)S(1)} %copy.32) | copy-start | bytes 6148
  26.1 6.7 %copy-start.12 = (f32[256]{0:T(256)S(1)}, f32[256]{0:T(256)}, u32[]{:S(2)}) copy-start(f32[256]{0:T(256)} %param.26) | copy-start | bytes 3076
  26.1 48.1 %all-to-all-start = ((bf16[4,1,8,24,2048]{4,3,2,1,0:T(8,128)(2,1)}), bf16[4,1,8,24,2048]{4,3,2,1,0:T(8,128)(2,1)}, u32[]{:S(2)}, u32[]{:S(2)}) async-start(bf16[4,1,8,24,2048]{4,3,2,1,0:T(8,128)(2,1)} %broadcast_select_fusion), calls=%async_computation | async-start | bytes 6291456 | tf_op jit(solution)/shard_map/all_to_all | solution.py:216
  31.4 3.5 %copy-start.9 = (bf16[1024,32]{0,1:T(8,128)(2,1)S(1)}, bf16[1024,32]{0,1:T(8,128)(2,1)}, u32[]{:S(2)}) copy-start(bf16[1024,32]{0,1:T(8,128)(2,1)} %param.24) | copy-start | bytes 196612
  31.4 5.1 %copy-start.14 = (bf16[512,192]{0,1:T(8,128)(2,1)S(1)}, bf16[512,192]{0,1:T(8,128)(2,1)}, u32[]{:S(2)}) copy-start(bf16[512,192]{0,1:T(8,128)(2,1)} %param.27) | copy-start | bytes 589828
  31.4 5.1 %copy-start.15 = (f32[512]{0:T(512)S(1)}, f32[512]{0:T(512)}, u32[]{:S(2)}) copy-start(f32[512]{0:T(512)} %param.25) | copy-start | bytes 6148
  31.4 70.1 %all-gather.2.cloned.1.call-start = ((), (), s32[]{:S(2)}) async-start(), calls=%async_computation.3 | async-start | bytes 2621440 | tf_op jit(solution)/shard_map/all_gather | solution.py:167
  34.9 144.6 %all-reduce.3.cloned.1.call-start = ((), (), s32[]{:S(2)}) async-start(), calls=%async_computation.5 | async-start | bytes 6291456
  38.3 0.9 copy-start.6
  87.9 129.7 %reduce-scatter.3.cloned.1.call-start = ((), (), s32[]{:S(2)}) async-start(), calls=%async_computation.4 | async-start | bytes 1179648 | tf_op jit(solution)/shard_map/reduce_scatter | solution.py:240
  88.0 12.3 %copy-start.4 = (bf16[2048,256]{1,0:T(8,128)(2,1)S(1)}, bf16[2048,256]{1,0:T(8,128)(2,1)}, u32[]{:S(2)}) copy-start(bf16[2048,256]{1,0:T(8,128)(2,1)} %param.37) | copy-start | bytes 3145732
  112.5 1.1 copy-start.7
  112.5 1.2 copy-start.1
  113.7 1.5 copy-start.8
  115.2 0.8 copy-start.2
  123.1 8.8 %copy-start.13 = (f32[256,2]{0,1:T(2,128)S(1)}, f32[256,2]{0,1:T(2,128)}, u32[]{:S(2)}) copy-start(f32[256,2]{0,1:T(2,128)} %param.33) | copy-start | bytes 6148
  123.1 9.6 %copy-start.16 = (u32[32]{0:T(128)S(1)}, u32[32]{0:T(128)}, u32[]{:S(2)}) copy-start(u32[32]{0:T(128)} %constant.155) | copy-start | bytes 388
  123.1 8.7 %collective-permute-start = (bf16[1024,128]{0,1:T(8,128)(2,1)S(1)}, bf16[1024,128]{0,1:T(8,128)(2,1)}, u32[]{:S(2)}, u32[]{:S(2)}) collective-permute-start(bf16[1024,128]{0,1:T(8,128)(2,1)S(1)} %bitcast.84), channel_id=1, source_target_pairs={{0,1},{1,2},{2,3},{3,4},{4,5},{5,6},{6,7},{7,0},{8,9},{9,10},{10,1... | collective-permute-start | bytes 786440 | tf_op jit(solution)/shard_map/ppermute | solution.py:25
  127.4 14.1 %collective-permute-start.1 = (bf16[1024,128]{0,1:T(8,128)(2,1)S(1)}, bf16[1024,128]{0,1:T(8,128)(2,1)S(1)}, u32[]{:S(2)}, u32[]{:S(2)}) collective-permute-start(bf16[1024,128]{0,1:T(8,128)(2,1)S(1)} %bitcast.85), channel_id=1, source_target_pairs={{0,7},{1,0},{2,1},{3,2},{4,3},{5,4},{6,5},{7,6},{8,15},{9,8},{10,9... | collective-permute-start | bytes 786440 | tf_op jit(solution)/shard_map/ppermute | solution.py:30
  131.8 17.4 %collective-permute-start.2 = (bf16[1024,128]{0,1:T(8,128)(2,1)}, bf16[1024,128]{0,1:T(8,128)(2,1)S(1)}, u32[]{:S(2)}, u32[]{:S(2)}) collective-permute-start(bf16[1024,128]{0,1:T(8,128)(2,1)} %collective-permute-done), channel_id=1, source_target_pairs={{0,1},{1,2},{2,3},{3,4},{4,5},{5,6},{6,7},{7,0},{8,9},{9,10},{10,1... | collective-permute-start | bytes 786440 | tf_op jit(solution)/shard_map/ppermute | solution.py:25
  141.5 16.1 %collective-permute-start.3 = (bf16[1024,128]{0,1:T(8,128)(2,1)S(1)}, bf16[1024,128]{0,1:T(8,128)(2,1)S(1)}, u32[]{:S(2)}, u32[]{:S(2)}) collective-permute-start(bf16[1024,128]{0,1:T(8,128)(2,1)S(1)} %collective-permute-done.1), channel_id=1, source_target_pairs={{0,7},{1,0},{2,1},{3,2},{4,3},{5,4},{6,5},{7,6},{8,15},{9,8},{10,9... | collective-permute-start | bytes 786440 | tf_op jit(solution)/shard_map/ppermute | solution.py:30
  149.2 16.1 %collective-permute-start.4 = (bf16[1024,128]{0,1:T(8,128)(2,1)S(1)}, bf16[1024,128]{0,1:T(8,128)(2,1)S(1)}, u32[]{:S(2)}, u32[]{:S(2)}) collective-permute-start(bf16[1024,128]{0,1:T(8,128)(2,1)S(1)} %collective-permute-done.2), channel_id=1, source_target_pairs={{0,1},{1,2},{2,3},{3,4},{4,5},{5,6},{6,7},{7,0},{8,9},{9,10},{10,1... | collective-permute-start | bytes 786440 | tf_op jit(solution)/shard_map/ppermute | solution.py:25
  157.6 36.7 %collective-permute-start.5 = (bf16[1024,128]{0,1:T(8,128)(2,1)S(1)}, bf16[1024,128]{0,1:T(8,128)(2,1)S(1)}, u32[]{:S(2)}, u32[]{:S(2)}) collective-permute-start(bf16[1024,128]{0,1:T(8,128)(2,1)S(1)} %collective-permute-done.3), channel_id=1, source_target_pairs={{0,7},{1,0},{2,1},{3,2},{4,3},{5,4},{6,5},{7,6},{8,15},{9,8},{10,9... | collective-permute-start | bytes 786440 | tf_op jit(solution)/shard_map/ppermute | solution.py:30
  165.4 29.6 %collective-permute-start.6 = (bf16[1024,128]{0,1:T(8,128)(2,1)S(1)}, bf16[1024,128]{0,1:T(8,128)(2,1)S(1)}, u32[]{:S(2)}, u32[]{:S(2)}) collective-permute-start(bf16[1024,128]{0,1:T(8,128)(2,1)S(1)} %collective-permute-done.4), channel_id=1, source_target_pairs={{0,1},{1,2},{2,3},{3,4},{4,5},{5,6},{6,7},{7,0},{8,9},{9,10},{10,1... | collective-permute-start | bytes 786440 | tf_op jit(solution)/shard_map/ppermute | solution.py:25
  181.9 17.6 %all-to-all-start.1 = ((bf16[4,1,1,24,2048]{4,3,2,1,0:T(8,128)(2,1)}), bf16[4,1,1,24,2048]{4,3,2,1,0:T(8,128)(2,1)S(1)}, u32[]{:S(2)}, u32[]{:S(2)}) async-start(bf16[4,1,1,24,2048]{4,3,2,1,0:T(8,128)(2,1)} %dynamic-slice_bitcast_fusion), calls=%async_computation.1 | async-start | bytes 786432 | tf_op jit(solution)/shard_map/all_to_all | solution.py:249
  199.5 1.1 copy-start.10
Sparse Core Ops, SparseCore 0:
  35.0 58.9 all-gather.1
Sparse Core Ops, SparseCore 1:
  88.0 91.4 all-reduce.2
  181.6 35.9 reduce-scatter.2
